TPU v7x, 32 devices: a whole 2x2x4 slice. The times are simulated.
32 devices in a mesh: sp: 8 (over z, y), tp: 4 (over x, core).
Axes of the slice: x: 2, y: 2, z: 4, core: 2. Of those that a mesh axis runs over, the one named last changes fastest.
Arguments:
- stream: bfloat16 [3072, 2048], P(('sp', 'tp')), may hold values from -6 to 6
- query_projected: bfloat16 [3072, 1024], P('sp', 'tp'), may hold values from -6 to 6
- key_projected: bfloat16 [3072, 1024], P('sp', 'tp'), may hold values from -6 to 6
- value_projected: bfloat16 [3072, 1024], P('sp', 'tp'), may hold values from -6 to 6
- gate_projected: bfloat16 [3072, 1024], P('sp', 'tp'), may hold values from -6 to 6
- strength_logits: bfloat16 [8, 3072], P('tp', 'sp'), may hold values from -7 to 4
- decay_preactivation: bfloat16 [8, 3072], P('tp', 'sp'), may hold values from -9 to 9
- extra_log_decay: float32 [8, 3072], P('tp', 'sp'), may hold values from -0.7 to 0
- head_decay_rate: float32 [8], P('tp'), may hold values from 0 to 0.1
- head_norm_gain: float32 [128], replicated, may hold values from 0.1 to 1.9
- head_output_matrix: bfloat16 [1024, 2048], P('tp'), may hold values from -0.1875 to 0.1875
- feed_norm_gain: float32 [2048], replicated, may hold values from 0.1 to 1.9
- gate_matrix: bfloat16 [2048, 5632], P('sp', 'tp'), may hold values from -0.125 to 0.125
- up_matrix: bfloat16 [2048, 5632], P('sp', 'tp'), may hold values from -0.125 to 0.125
- down_matrix: bfloat16 [5632, 2048], P('tp', 'sp'), may hold values from -0.078125 to 0.078125
Outputs:
- result: bfloat16 [3072, 2048], P(('sp', 'tp'))
All inputs are finite; a program needn't handle non-finite values.
Results may differ from a plain program's by a relative error of at most 0.015.
Values may be sent and summed in bfloat16 or wider, within the bound.
A program may use at most 128 MiB of HBM per device.

v0:
```python
import jax
import jax.numpy as jnp
from jax import lax
from jax.sharding import PartitionSpec as P

HEAD = 128
BLOCK = 64


PRECISION_FULL = lax.Precision.HIGHEST
EPSILON = 1e-06


def from_behind(value, axis, by):
    size = lax.axis_size(axis)
    pairs = [(i, i + by) for i in range(size) if 0 <= i + by < size]
    return lax.ppermute(value, axis, pairs)


def unit_rows(tensor):
    return tensor * lax.rsqrt(jnp.sum(tensor * tensor, axis=-1, keepdims=True) + EPSILON)


def rms_scale(tensor):
    return tensor * lax.rsqrt(jnp.mean(tensor * tensor, axis=-1, keepdims=True) + EPSILON)


def block_correction(
    unit_queries,
    unit_keys,
    complete_values,
    strength_logits,
    decay_preactivation,
    extra_log_decay,
    head_decay_rate,
):
    head_count, length, head_width = unit_queries.shape
    block_count = length // BLOCK

    def to_blocks(tensor):
        return tensor.reshape((head_count, block_count, BLOCK) + tensor.shape[2:])

    beta_gate = jax.nn.sigmoid(strength_logits.astype(jnp.float32))
    decay_logarithm = (
        -head_decay_rate[:, None] * jax.nn.softplus(decay_preactivation.astype(jnp.float32))
        + extra_log_decay
    )
    query_block = to_blocks(unit_queries)
    key_block = to_blocks(unit_keys)
    value_block = to_blocks(complete_values)
    beta_block = to_blocks(beta_gate)
    cumulative = jnp.cumsum(to_blocks(decay_logarithm), axis=-1)
    causal = jnp.tril(jnp.ones((BLOCK, BLOCK), bool))
    strict = jnp.tril(jnp.ones((BLOCK, BLOCK), bool), -1)
    spread = cumulative[..., :, None] - cumulative[..., None, :]
    damping = jnp.where(causal, jnp.exp(jnp.where(causal, spread, 0.0)), 0.0)
    key_beta = key_block * beta_block[..., None]
    lower_part = jnp.einsum(
        "hnid,hnjd->hnij", key_beta, key_block, precision=PRECISION_FULL
    ) * jnp.where(strict, damping, 0.0)
    system = lower_part + jnp.eye(BLOCK, dtype=jnp.float32)
    right_side = jnp.concatenate(
        [value_block * beta_block[..., None], key_beta * jnp.exp(cumulative)[..., None]], axis=-1
    )
    solved = lax.linalg.triangular_solve(
        system, right_side, left_side=True, lower=True, unit_diagonal=True
    )
    target_values = solved[..., :head_width]
    householder_weights = solved[..., head_width:]
    inner_scores = (
        jnp.einsum("hnid,hnjd->hnij", query_block, key_block, precision=PRECISION_FULL) * damping
    )
    decayed_queries = query_block * jnp.exp(cumulative)[..., None]
    closing_log_decay = cumulative[..., -1:]
    decayed_keys = key_block * jnp.exp(closing_log_decay - cumulative)[..., None]
    return (
        decayed_queries,
        decayed_keys,
        target_values,
        householder_weights,
        inner_scores,
        closing_log_decay,
    )


def local_recurrence(
    query_projected,
    key_projected,
    value_projected,
    strength_logits,
    decay_preactivation,
    extra_log_decay,
    head_decay_rate,
):
    head_count = strength_logits.shape[0]
    tok_count = strength_logits.shape[1]

    def split_heads(tensor):
        return tensor.reshape(tok_count, head_count, HEAD).transpose(1, 0, 2).astype(jnp.float32)

    unit_queries = unit_rows(split_heads(query_projected)) * HEAD ** (-0.5)
    unit_keys = unit_rows(split_heads(key_projected))
    complete_values = split_heads(value_projected)
    score_terms = block_correction(
        unit_queries,
        unit_keys,
        complete_values,
        strength_logits,
        decay_preactivation,
        extra_log_decay,
        head_decay_rate,
    )
    identity = jnp.broadcast_to(jnp.eye(HEAD, dtype=jnp.float32), (head_count, HEAD, HEAD))

    def advance(carry, items):
        running_state, matrix_product = carry
        (
            decayed_queries,
            decayed_keys,
            target_values,
            householder_weights,
            inner_scores,
            closing_log_decay,
        ) = items
        new_state = target_values - jnp.einsum(
            "fdc,fcj->fdj", householder_weights, running_state, precision=PRECISION_FULL
        )
        layer_output = jnp.einsum(
            "fdc,fcj->fdj", decayed_queries, running_state, precision=PRECISION_FULL
        )
        layer_output = layer_output + jnp.einsum(
            "hij,hjv->hiv", inner_scores, new_state, precision=PRECISION_FULL
        )
        passed_state = decayed_queries - jnp.einsum(
            "hij,hjk->hik", inner_scores, householder_weights, precision=PRECISION_FULL
        )
        decay_span = jnp.einsum(
            "fdc,fcj->fdj", passed_state, matrix_product, precision=PRECISION_FULL
        )
        decay_factor = jnp.exp(closing_log_decay)[:, :, None]
        step_map = decay_factor * identity - jnp.einsum(
            "hik,hij->hkj", decayed_keys, householder_weights, precision=PRECISION_FULL
        )
        running_state = decay_factor * running_state + jnp.einsum(
            "xwp,xws->xps", decayed_keys, new_state, precision=PRECISION_FULL
        )
        matrix_product = jnp.einsum(
            "hij,hjk->hik", step_map, matrix_product, precision=PRECISION_FULL
        )
        return ((running_state, matrix_product), (layer_output, decay_span))

    moved = tuple((jnp.moveaxis(tensor, 1, 0) for tensor in score_terms))
    zeros_state = jnp.zeros((head_count, HEAD, HEAD), jnp.float32)
    (running_state, matrix_product), (block_outputs, decay_spans) = lax.scan(
        advance, (zeros_state, identity), moved
    )

    def merge_blocks(tensor):
        return jnp.moveaxis(tensor, 0, 1).reshape(head_count, tok_count, HEAD)

    return (
        merge_blocks(block_outputs),
        merge_blocks(decay_spans),
        matrix_product,
        running_state,
        identity,
    )


def feed_forward(whole_rows, gate_matrix, up_matrix, down_matrix):
    gate_whole, up_whole = (
        lax.all_gather(gate_matrix, "sp", axis=0, tiled=True),
        lax.all_gather(up_matrix, "sp", axis=0, tiled=True),
    )
    gate_total = jnp.dot(whole_rows, gate_whole, preferred_element_type=jnp.float32)
    up_total = jnp.dot(whole_rows, up_whole, preferred_element_type=jnp.float32)
    hidden = (jax.nn.silu(gate_total) * up_total).astype(jnp.bfloat16)
    down_whole = lax.all_gather(down_matrix, "sp", axis=1, tiled=True)
    return jnp.dot(hidden, down_whole, preferred_element_type=jnp.float32)


def body(
    stream,
    query_projected,
    key_projected,
    value_projected,
    gate_projected,
    strength_logits,
    decay_preactivation,
    extra_log_decay,
    head_decay_rate,
    head_norm_gain,
    head_output_matrix,
    feed_norm_gain,
    gate_matrix,
    up_matrix,
    down_matrix,
):
    block_outputs, decay_spans, matrix_product, running_state, identity = local_recurrence(
        query_projected,
        key_projected,
        value_projected,
        strength_logits,
        decay_preactivation,
        extra_log_decay,
        head_decay_rate,
    )
    zeros_state = jnp.zeros_like(running_state)

    def pass_state(turn, state_inflow):
        leaving = (
            jnp.einsum("hij,hjk->hik", matrix_product, state_inflow, precision=PRECISION_FULL)
            + running_state
        )
        return from_behind(leaving.astype(jnp.bfloat16), "sp", 1).astype(leaving.dtype)

    state_inflow = lax.fori_loop(0, lax.axis_size("sp") - 1, pass_state, zeros_state)
    attention_output = block_outputs + jnp.einsum(
        "qwc,qcn->qwn", decay_spans, state_inflow, precision=PRECISION_FULL
    )
    head_count = attention_output.shape[0]
    tok_count = attention_output.shape[1]
    normed_heads = rms_scale(attention_output) * head_norm_gain
    gated = normed_heads.transpose(1, 0, 2).reshape(tok_count, head_count * HEAD)
    mixed = (gated * jax.nn.silu(gate_projected.astype(jnp.float32))).astype(jnp.bfloat16)
    branch = lax.psum_scatter(
        jnp.dot(mixed, head_output_matrix, preferred_element_type=jnp.float32).astype(jnp.bfloat16),
        "tp",
        scatter_dimension=0,
        tiled=True,
    ).astype(jnp.float32)
    residual_own = stream.astype(jnp.float32) + branch
    normed_own = (rms_scale(residual_own) * feed_norm_gain).astype(jnp.bfloat16)
    whole_rows = lax.all_gather(normed_own, "tp", axis=0, tiled=True)
    ffn_term = feed_forward(whole_rows, gate_matrix, up_matrix, down_matrix)
    ffn_own = lax.psum_scatter(
        ffn_term.astype(jnp.bfloat16), "tp", scatter_dimension=0, tiled=True
    ).astype(jnp.float32)
    return (residual_own + ffn_own).astype(jnp.bfloat16)


def solution(mesh):
    placed = (
        P(("sp", "tp"), None),
        P("sp", "tp"),
        P("sp", "tp"),
        P("sp", "tp"),
        P("sp", "tp"),
        P("tp", "sp"),
        P("tp", "sp"),
        P("tp", "sp"),
        P("tp"),
        P(),
        P("tp", None),
        P(),
        P("sp", "tp"),
        P("sp", "tp"),
        P("tp", "sp"),
    )
    return jax.shard_map(
        body, mesh=mesh, in_specs=placed, out_specs=P(("sp", "tp"), None), check_vma=False
    )
```

profile of v0, /device:TPU:0, one launch (start us, length us, event | category | flops | bytes accessed | tf_op | source)
XLA Modules:
  0.0 551.2 jit_solution(7347479485389619198)
XLA Ops:
  8.9 1.1 fusion.64
  11.1 1.1 fusion.60
  16.0 59.6 %custom-call.3 = f32[2,6,1,64,64]{3,4,2,1,0:T(8,128)} custom-call(f32[2,6,1,64,64]{4,3,2,1,0:T(8,128)S(1)} %fusion.48), custom_call_target="InvertDiagBlocksLowerTriangular" | custom-call | tf_op jit(solution)/shard_map/triangular_solve | solution.py:65
  79.3 36.4 %while.28 = (s32[]{:T(128)}, f32[2,128,128]{2,1,0:T(8,128)S(1)}, f32[2,128,128]{2,1,0:T(8,128)S(1)}, f32[6,2,64,128]{3,2,0,1:T(8,128)}, f32[6,2,64,128]{3,2,0,1:...) while((s32[]{:T(128)}, f32[2,128,128]{2,1,0:T(8,128)S(1)}, ...), condition=%wide.region_4.5_spmd.clone, body=%wide.region_3.4_spmd.clone.sunk | while | flops 201605120 | bytes 2759337 | solution.py:154
  115.7 1.2 copy.42
  116.9 49.8 %while.29 = (s32[]{:T(128)}, f32[2,128,128]{2,1,0:T(8,128)S(1)}, f32[2,128,128]{2,1,0:T(8,128)S(1)}, f32[2,128,128]{2,1,0:T(8,128)S(1)}, s32[]{:T(128)}, /*index=5*/s32[]{:T(128)}) while((s32[]{:T(128)}, f32[2,128,128]{2,1,0:T(8,128)S(1)}, f32[2,128,128]{2,1,0:T(8,128)S(1)}, f32[2,128,128]{2,1,0:T(8,128)S(1)}, s32[]{:T(128)}, ...), condition=%wide.region_6.7_spmd.clone, body=%wide.region_5.6_spmd.clone.sunk | while | flops 50462720 | bytes 917623 | solution.py:217
  117.2 4.9 collective-permute-start
  122.1 1.9 collective-permute-done
  124.3 4.3 collective-permute-start
  128.6 1.9 collective-permute-done
  130.8 4.3 collective-permute-start
  135.1 1.9 collective-permute-done
  137.3 5.2 collective-permute-start
  142.5 1.9 collective-permute-done
  144.7 5.2 collective-permute-start
  149.9 1.9 collective-permute-done
  152.1 5.3 collective-permute-start
  157.3 2.1 collective-permute-done
  159.7 5.1 collective-permute-start
  164.8 1.9 collective-permute-done
  167.8 1.8 convolution_convert_fusion.1
  169.6 31.9 %reduce-scatter.3.cloned.1.call-done = bf16[96,2048]{1,0:T(8,128)(2,1)} async-done(((bf16[384,2048]{1,0:T(8,128)(2,1)}), bf16[96,2048]{1,0:T(8,128)(2,1)}) %reduce-scatter.3.cloned.1.call-update) | async-done | bytes 393232 | tf_op jit(solution)/shard_map/reduce_scatter | solution.py:226
  201.5 1.2 multiply_reduce_fusion
  202.8 1.9 multiply_convert_fusion
  206.8 17.7 %all-gather.5.cloned.1.call-done = bf16[384,2048]{1,0:T(8,128)(2,1)} async-done(((bf16[96,2048]{1,0:T(8,128)(2,1)}), bf16[384,2048]{1,0:T(8,128)(2,1)}) %all-gather.5.cloned.1.call-update) | async-done | bytes 1572880 | tf_op jit(solution)/shard_map/all_gather | solution.py:234
  224.5 94.5 %all-gather.7.cloned.1.call-done = bf16[2048,1408]{1,0:T(8,128)(2,1)} async-done(((bf16[256,1408]{1,0:T(8,128)(2,1)}), bf16[2048,1408]{1,0:T(8,128)(2,1)}) %all-gather.7.cloned.1.call-update) | async-done | bytes 5767184 | tf_op jit(solution)/shard_map/all_gather | solution.py:172
  319.0 7.1 %fusion.84 = f32[384,1408]{1,0:T(8,128)} fusion(bf16[384,2048]{1,0:T(8,128)(2,1)} %all-gather.5.cloned.1.call-done, bf16[2048,1408]{1,0:T(8,128)(2,1)} %all-gather.7.cloned.1.call-done), kind=kOutput, calls=%fused_computation.133 | convolution fusion | flops 2214592512 | bytes 9502720 | tf_op jit(solution)/shard_map/dot_general | solution.py:175
  326.1 86.2 %all-gather.11.cloned.1.call-done = bf16[1408,2048]{1,0:T(8,128)(2,1)} async-done(((bf16[1408,256]{1,0:T(8,128)(2,1)}), bf16[1408,2048]{1,0:T(8,128)(2,1)}) %all-gather.11.cloned.1.call-update) | async-done | bytes 5767184 | tf_op jit(solution)/shard_map/all_gather | solution.py:178
  412.3 92.6 %all-gather.9.cloned.1.call-done = bf16[2048,1408]{1,0:T(8,128)(2,1)} async-done(((bf16[256,1408]{1,0:T(8,128)(2,1)}), bf16[2048,1408]{1,0:T(8,128)(2,1)}) %all-gather.9.cloned.1.call-update) | async-done | bytes 5767184 | tf_op jit(solution)/shard_map/all_gather | solution.py:173
  504.8 11.3 %convolution_convert_fusion = bf16[384,2048]{1,0:T(8,128)(2,1)} fusion(bf16[1408,2048]{1,0:T(8,128)(2,1)} %all-gather.11.cloned.1.call-done, bf16[384,2048]{1,0:T(8,128)(2,1)S(1)} %copy-done.7, bf16[2048,1408]{1,0:T(8,128)(2,1)} %all-gather.9.cloned.1.call-done, f32[384,1408]{1,0:T(8,128)} %fusion.84), kind=kOutput, calls=%fused_computation.52 | convolution fusion | flops 4433215488 | bytes 16842752 | tf_op jit(solution)/shard_map/dot_general | solution.py:179
  516.1 26.4 %reduce-scatter.5.cloned.1.call-done = bf16[96,2048]{1,0:T(8,128)(2,1)} async-done(((bf16[384,2048]{1,0:T(8,128)(2,1)}), bf16[96,2048]{1,0:T(8,128)(2,1)}) %reduce-scatter.5.cloned.1.call-update) | async-done | bytes 393232 | tf_op jit(solution)/shard_map/reduce_scatter | solution.py:236
  542.5 1.9 add_convert_fusion
  (137 shorter events, 51.8 us)
Async XLA Ops:
  6.5 161.2 %copy-start = (bf16[256,2048]{1,0:T(8,128)(2,1)S(1)}, bf16[256,2048]{1,0:T(8,128)(2,1)}, u32[]{:S(2)}) copy-start(bf16[256,2048]{1,0:T(8,128)(2,1)} %param.29) | copy-start | bytes 3145732
  6.5 195.0 %reduce-scatter.3.cloned.1.call-start = ((), (), s32[]{:S(2)}) async-start(), calls=%async_computation.2 | async-start | bytes 1966080 | tf_op jit(solution)/shard_map/reduce_scatter | solution.py:226
  75.6 1.1 copy-start.4
  115.7 51.0 %copy-start.3 = (f32[6,2,64,128]{3,2,0,1:T(8,128)S(1)}, f32[6,2,64,128]{3,2,0,1:T(8,128)}, u32[]{:S(2)}) copy-start(f32[6,2,64,128]{3,2,0,1:T(8,128)} %get-tuple-element.93) | copy-start | bytes 1179652
  116.9 50.5 %copy-start.6 = (f32[128]{0:T(128)S(1)}, f32[128]{0:T(128)}, u32[]{:S(2)}) copy-start(f32[128]{0:T(128)} %param.28) | copy-start | bytes 1540
  117.2 6.8 %collective-permute-start = (bf16[2,128,128]{2,1,0:T(8,128)(2,1)S(1)}, bf16[2,128,128]{2,1,0:T(8,128)(2,1)S(1)}, u32[]{:S(2)}, u32[]{:S(2)}) collective-permute-start(bf16[2,128,128]{2,1,0:T(8,128)(2,1)S(1)} %fusion.150), channel_id=1, source_target_pairs={{0,4},{4,8},{8,12},{12,16},{16,20},{20,24},{24,28},{1,5},{5,9},{9,... | collective-permute-start | bytes 196616 | tf_op jit(solution)/shard_map/while/body/eval_jaxpr/ppermute | solution.py:17
  124.3 6.2 %collective-permute-start = (bf16[2,128,128]{2,1,0:T(8,128)(2,1)S(1)}, bf16[2,128,128]{2,1,0:T(8,128)(2,1)S(1)}, u32[]{:S(2)}, u32[]{:S(2)}) collective-permute-start(bf16[2,128,128]{2,1,0:T(8,128)(2,1)S(1)} %fusion.150), channel_id=1, source_target_pairs={{0,4},{4,8},{8,12},{12,16},{16,20},{20,24},{24,28},{1,5},{5,9},{9,... | collective-permute-start | bytes 196616 | tf_op jit(solution)/shard_map/while/body/eval_jaxpr/ppermute | solution.py:17
  130.8 6.2 %collective-permute-start = (bf16[2,128,128]{2,1,0:T(8,128)(2,1)S(1)}, bf16[2,128,128]{2,1,0:T(8,128)(2,1)S(1)}, u32[]{:S(2)}, u32[]{:S(2)}) collective-permute-start(bf16[2,128,128]{2,1,0:T(8,128)(2,1)S(1)} %fusion.150), channel_id=1, source_target_pairs={{0,4},{4,8},{8,12},{12,16},{16,20},{20,24},{24,28},{1,5},{5,9},{9,... | collective-permute-start | bytes 196616 | tf_op jit(solution)/shard_map/while/body/eval_jaxpr/ppermute | solution.py:17
  137.3 7.1 %collective-permute-start = (bf16[2,128,128]{2,1,0:T(8,128)(2,1)S(1)}, bf16[2,128,128]{2,1,0:T(8,128)(2,1)S(1)}, u32[]{:S(2)}, u32[]{:S(2)}) collective-permute-start(bf16[2,128,128]{2,1,0:T(8,128)(2,1)S(1)} %fusion.150), channel_id=1, source_target_pairs={{0,4},{4,8},{8,12},{12,16},{16,20},{20,24},{24,28},{1,5},{5,9},{9,... | collective-permute-start | bytes 196616 | tf_op jit(solution)/shard_map/while/body/eval_jaxpr/ppermute | solution.py:17
  144.7 7.1 %collective-permute-start = (bf16[2,128,128]{2,1,0:T(8,128)(2,1)S(1)}, bf16[2,128,128]{2,1,0:T(8,128)(2,1)S(1)}, u32[]{:S(2)}, u32[]{:S(2)}) collective-permute-start(bf16[2,128,128]{2,1,0:T(8,128)(2,1)S(1)} %fusion.150), channel_id=1, source_target_pairs={{0,4},{4,8},{8,12},{12,16},{16,20},{20,24},{24,28},{1,5},{5,9},{9,... | collective-permute-start | bytes 196616 | tf_op jit(solution)/shard_map/while/body/eval_jaxpr/ppermute | solution.py:17
  152.1 7.4 %collective-permute-start = (bf16[2,128,128]{2,1,0:T(8,128)(2,1)S(1)}, bf16[2,128,128]{2,1,0:T(8,128)(2,1)S(1)}, u32[]{:S(2)}, u32[]{:S(2)}) collective-permute-start(bf16[2,128,128]{2,1,0:T(8,128)(2,1)S(1)} %fusion.150), channel_id=1, source_target_pairs={{0,4},{4,8},{8,12},{12,16},{16,20},{20,24},{24,28},{1,5},{5,9},{9,... | collective-permute-start | bytes 196616 | tf_op jit(solution)/shard_map/while/body/eval_jaxpr/ppermute | solution.py:17
  159.7 7.0 %collective-permute-start = (bf16[2,128,128]{2,1,0:T(8,128)(2,1)S(1)}, bf16[2,128,128]{2,1,0:T(8,128)(2,1)S(1)}, u32[]{:S(2)}, u32[]{:S(2)}) collective-permute-start(bf16[2,128,128]{2,1,0:T(8,128)(2,1)S(1)} %fusion.150), channel_id=1, source_target_pairs={{0,4},{4,8},{8,12},{12,16},{16,20},{20,24},{24,28},{1,5},{5,9},{9,... | collective-permute-start | bytes 196616 | tf_op jit(solution)/shard_map/while/body/eval_jaxpr/ppermute | solution.py:17
  166.7 1.0 copy-start.8
  167.7 33.8 %copy-start.1 = (bf16[96,2048]{1,0:T(8,128)(2,1)S(1)}, bf16[96,2048]{1,0:T(8,128)(2,1)}, u32[]{:S(2)}) copy-start(bf16[96,2048]{1,0:T(8,128)(2,1)} %param.19) | copy-start | bytes 1179652
  167.7 35.0 %copy-start.5 = (f32[2048]{0:T(1024)S(1)}, f32[2048]{0:T(1024)}, u32[]{:S(2)}) copy-start(f32[2048]{0:T(1024)} %param.30) | copy-start | bytes 24580
  169.6 54.9 %all-gather.5.cloned.1.call-start = ((), (), s32[]{:S(2)}) async-start(), calls=%async_computation.3 | async-start | bytes 1966080 | tf_op jit(solution)/shard_map/all_gather | solution.py:234
  204.7 114.3 %all-gather.7.cloned.1.call-start = ((), (), s32[]{:S(2)}) async-start(), calls=%async_computation.4 | async-start | bytes 6488064 | tf_op jit(solution)/shard_map/all_gather | solution.py:172
  205.4 206.8 %all-gather.11.cloned.1.call-start = ((), (), s32[]{:S(2)}) async-start(), calls=%async_computation.6 | async-start | bytes 6488064 | tf_op jit(solution)/shard_map/all_gather | solution.py:178
  206.0 298.8 %all-gather.9.cloned.1.call-start = ((), (), s32[]{:S(2)}) async-start(), calls=%async_computation.5 | async-start | bytes 6488064 | tf_op jit(solution)/shard_map/all_gather | solution.py:173
  206.6 335.9 %reduce-scatter.5.cloned.1.call-start = ((), (), s32[]{:S(2)}) async-start(), calls=%async_computation.7 | async-start | bytes 1966080 | tf_op jit(solution)/shard_map/reduce_scatter | solution.py:236
  224.5 280.3 %copy-start.7 = (bf16[384,2048]{1,0:T(8,128)(2,1)S(1)}, bf16[384,2048]{1,0:T(8,128)(2,1)}, u32[]{:S(2)}) copy-start(bf16[384,2048]{1,0:T(8,128)(2,1)} %all-gather.5.cloned.1.call-done) | copy-start | bytes 4718596
  326.1 216.4 %copy-start.2 = (bf16[96,2048]{1,0:T(8,128)(2,1)S(1)}, bf16[96,2048]{1,0:T(8,128)(2,1)}, u32[]{:S(2)}) copy-start(bf16[96,2048]{1,0:T(8,128)(2,1)} %reduce-scatter.3.cloned.1.call-done) | copy-start | bytes 1179652
Sparse Core Ops, SparseCore 0:
  169.7 31.7 reduce-scatter.2
  204.8 19.6 all-gather.4
  226.7 92.3 all-gather.6
  320.9 91.2 all-gather.10
  414.3 90.4 all-gather.8
  516.2 26.1 reduce-scatter.4
where the time goes:
time: 553 us; the launch traced here: 551 us
  waiting for transfers between devices  364 us (66%)
  other arithmetic  74.1 us (13%)
  matrix products  60.9 us (11%)
  starting transfers between devices  34.5 us (6%)
  between operations  13.7 us (2%)
    all_gather x1, waiting for transfers between devices, feed_forward(): lax.all_gather(gate_matrix, 'sp', axis=0, tiled=True)  94.5 us
    all_gather x1, waiting for transfers between devices, feed_forward(): lax.all_gather(up_matrix, 'sp', axis=0, tiled=True)  92.6 us
    all_gather x1, waiting for transfers between devices, feed_forward(): down_whole = lax.all_gather(down_matrix, 'sp', axis=1, tiled=True)  86.2 us
    another operation x2, other arithmetic, block_correction(): lax.linalg.triangular_solve(system, right_side, left_side=True, lower=Tru...  59.6 us
    ppermute x7, starting transfers between devices, from_behind(): return lax.ppermute(value, axis, pairs)  34.2 us
    reduce_scatter x1, waiting for transfers between devices, body(): lax.psum_scatter(jnp.dot(mixed, head_output_matrix, preferred_element_typ...  31.9 us
    reduce_scatter x1, waiting for transfers between devices, body(): lax.psum_scatter(ffn_term.astype(jnp.bfloat16), 'tp', scatter_dimension=0...  26.4 us
    all_gather x1, waiting for transfers between devices, body(): whole_rows = lax.all_gather(normed_own, 'tp', axis=0, tiled=True)  17.7 us
  transfers between devices with their start and end apart: 13, of which 13 were waited for; matrix products, arithmetic and copies ran while one was open for 1% of the time, Pallas kernels for 0%

commit v1 on v0

v1 whole, which is shorter than its diff:
```python
import functools

import jax
import jax.numpy as jnp
from jax import lax
from jax.experimental import pallas as pl
from jax.experimental.pallas import tpu as pltpu
from jax.sharding import PartitionSpec as P

HEAD = 128
CHUNK = 128
EPSILON = 1e-06
F32 = jnp.float32
BF16 = jnp.bfloat16
HIGHEST = lax.Precision.HIGHEST
NN = (((1,), (0,)), ((), ()))
NT = (((1,), (1,)), ((), ()))
TN = (((0,), (0,)), ((), ()))


def dot1(a, b, dims=NN):
    return lax.dot_general(a, b, dims, preferred_element_type=F32)


def halves(x):
    high = x.astype(BF16)
    return high, (x - high.astype(F32)).astype(BF16)


def dot3(a, b, dims=NN):
    ah, al = halves(a)
    bh, bl = halves(b)
    return dot1(ah, bh, dims) + (dot1(ah, bl, dims) + dot1(al, bh, dims))


def silu(x):
    return x * jax.nn.sigmoid(x)


def messages(ring):
    half = ring // 2
    first, relay_gate, relay_up, relay_down, late = [], [], [], [], []
    for a in "GU":
        for way in "RLY":
            first.append((a, 0, 0, way))
    for k in range(2, half + 1):
        relay_gate.append(("G", -(k - 1), 0, "R"))
        if k < half:
            relay_gate.append(("G", k - 1, 0, "L"))
    for k in range(1, half):
        relay_gate.append(("G", -k, 0, "Y"))
        relay_gate.append(("G", k, 0, "Y"))
    far_gate = [("G", half, 0, "Y")] if half else []
    for k in range(1, half + 1):
        for rel in (1, 0):
            if (k > 1 or rel == 1) and (k < half or rel == 0):
                relay_up.append(("U", -(k - 1), rel, "R"))
            if (k > 1 or rel == 1) and (k < half or rel == 1):
                relay_up.append(("U", k - 1, rel, "L"))
    down_own = [("D", 0, 0, way) for way in "RLY"]
    for k in range(1, half + 1):
        for rel in (1, 0):
            if (k > 1 or rel == 1) and k < half:
                relay_down.append(("D", -(k - 1), rel, "R"))
            if (k > 1 or rel == 1) and (k < half or rel == 0):
                relay_down.append(("D", k - 1, rel, "L"))
    late.append(("D", half, 0, "Y"))
    return first, relay_gate, far_gate, relay_up, down_own, relay_down, late


def kernel(
    n, tps, groups,
    stream, qp, kp, vp, gp, strength, decay_pre, extra, rate, head_gain, w_out, feed_gain,
    gate_in, up_in, down_in,
    result,
    gate_all, up_all, down_all, out_scr, x_send, x_part, p_send, p_recv, s_in, mixed,
    d_send, d_recv, residual, rows_all, hidden, f_part, f_recv,
    w_send, w_recv, own_sem, x_sem, p_ssem, p_rsem, d_ssem, d_rsem, e_ssem, e_rsem, f_ssem, f_rsem,
):
    ring = n // 2
    sp = lax.axis_index("sp")
    tp = lax.axis_index("tp")
    r = sp // 2
    p = lax.rem(sp, 2)
    heads = strength.shape[0]
    tokens = strength.shape[1]
    chunks = tokens // CHUNK
    own_rows = stream.shape[0]
    kr = gate_in.shape[0]
    MESH = pl.DeviceIdType.MESH

    def sp_of(dr, rel):
        q = p if rel == 0 else 1 - p
        return lax.rem(r + dr + ring, ring) * 2 + q

    partner = sp_of(0, 1)
    where = {"R": sp_of(1, 0), "L": sp_of(-1, 0), "Y": partner}

    def tp_peer(o):
        return lax.rem(tp + o, tps)

    barrier = pltpu.get_barrier_semaphore()
    for dr in range(1, ring):
        pl.semaphore_signal(barrier, 1, device_id=(sp_of(dr, 0), tp), device_id_type=MESH)
    pl.semaphore_signal(barrier, 1, device_id=(partner, tp), device_id_type=MESH)
    for o in range(1, tps):
        pl.semaphore_signal(barrier, 1, device_id=(sp, tp_peer(o)), device_id_type=MESH)
    pl.semaphore_wait(barrier, ring + tps - 1)

    flat = [m for g in groups for m in g]
    number = {m: i for i, m in enumerate(flat)}
    arrival = {}
    for (a, dr, rel, way) in flat:
        to = {"R": (dr - 1, rel), "L": (dr + 1, rel), "Y": (dr, 1 - rel)}[way]
        key = (a, to[0] % ring, to[1])
        assert key not in arrival
        arrival[key] = number[(a, dr, rel, way)]
    waited = set()
    copies = []

    def slot(a, dr, rel):
        s = sp_of(dr, rel)
        if a == "D":
            return down_all.at[s]
        whole = gate_all if a == "G" else up_all
        return whole.at[pl.ds(pl.multiple_of(s * kr, kr), kr), :]

    inputs = {"G": gate_in, "U": up_in, "D": down_in}

    def need(a, dr, rel):
        dr = dr % ring
        key = (a, dr, rel)
        if (dr == 0 and rel == 0) or key in waited:
            return
        waited.add(key)
        m = arrival[key]
        here = slot(*key)
        pltpu.make_async_remote_copy(
            here, here, w_send.at[m], w_recv.at[m], device_id=(partner, tp), device_id_type=MESH
        ).wait_recv()

    def pump(group):
        for message in group:
            a, dr, rel, way = message
            need(a, dr, rel)
            own = dr % ring == 0 and rel == 0
            m = number[message]
            copy = pltpu.make_async_remote_copy(
                inputs[a] if own else slot(a, dr % ring, rel),
                slot(a, dr % ring, rel),
                w_send.at[m], w_recv.at[m],
                device_id=(where[way], tp), device_id_type=MESH,
            )
            copy.start()
            copies.append(copy)

    first, relay_gate, far_gate, relay_up, down_own, relay_down, late = groups
    pump(first)
    locals_ = []
    for i, a in enumerate("GUD"):
        local = pltpu.make_async_copy(inputs[a], slot(a, 0, 0), own_sem.at[i])
        local.start()
        locals_.append(local)

    row_i = lax.broadcasted_iota(jnp.int32, (CHUNK, CHUNK), 0)
    col_i = lax.broadcasted_iota(jnp.int32, (CHUNK, CHUNK), 1)
    causal = row_i >= col_i
    strict = row_i > col_i
    eye = jnp.where(row_i == col_i, 1.0, 0.0).astype(F32)
    lower = jnp.where(causal, 1.0, 0.0).astype(F32)
    beta = jax.nn.sigmoid(strength[...].astype(F32))
    pre = decay_pre[...].astype(F32)
    soft = jnp.maximum(pre, 0.0) + jnp.log1p(jnp.exp(-jnp.abs(pre)))
    log_decay = -rate[...] * soft + extra[...]

    pairs = [(h, c) for c in range(chunks) for h in range(heads)]
    data = {}
    for c in range(chunks):
        span = slice(c * CHUNK, (c + 1) * CHUNK)
        ld = log_decay[:, span]
        c_row = lax.dot_general(ld, lower, NT, precision=HIGHEST, preferred_element_type=F32)
        c_col = lax.dot_general(lower, ld, NT, precision=HIGHEST, preferred_element_type=F32)
        b_col = lax.dot_general(eye, beta[:, span], NT, precision=HIGHEST, preferred_element_type=F32)
        for h in range(heads):
            lanes = slice(h * HEAD, (h + 1) * HEAD)
            q = qp[span, lanes].astype(F32)
            k = kp[span, lanes].astype(F32)
            v = vp[span, lanes].astype(F32)
            q = q * (lax.rsqrt(jnp.sum(q * q, axis=-1, keepdims=True) + EPSILON) * HEAD ** (-0.5))
            k = k * lax.rsqrt(jnp.sum(k * k, axis=-1, keepdims=True) + EPSILON)
            cc = c_col[:, h:h + 1]
            bb = b_col[:, h:h + 1]
            cr = c_row[h:h + 1, :]
            last = cr[:, CHUNK - 1:]
            damp = jnp.where(causal, jnp.exp(jnp.where(causal, cc - cr, 0.0)), 0.0)
            grown = jnp.exp(cc)
            kb = k * bb
            kk = dot3(kb, k, NT) * jnp.where(strict, damp, 0.0)
            inner = dot3(q, k, NT) * damp
            data[h, c] = dict(
                low=kk, inner=inner, v=v * bb, kw=kb * grown, qd=q * grown,
                kd=k * jnp.exp(last - cc), decay=jnp.exp(last),
            )
    inverse = {}
    b = 1
    shift = 0
    while b < CHUNK:
        mask = ((row_i >> (shift + 1)) == (col_i >> (shift + 1))) & (
            ((row_i >> shift) & 1) == 1) & (((col_i >> shift) & 1) == 0)
        for key in pairs:
            piece = jnp.where(mask, data[key]["low"], 0.0)
            if b == 1:
                inverse[key] = eye - piece
            else:
                x = inverse[key]
                inverse[key] = x - dot3(x, dot3(piece, x))
        b *= 2
        shift += 1
    states = [jnp.concatenate([jnp.zeros((HEAD, HEAD), F32), eye], axis=1) for _ in range(heads)]
    for c in range(chunks):
        for h in range(heads):
            e = data[h, c]
            u = dot3(inverse[h, c], e["v"])
            w = dot3(inverse[h, c], e["kw"])
            x = states[h]
            new = jnp.concatenate([u, jnp.zeros_like(u)], axis=1) - dot3(w, x)
            out_scr[h, c * CHUNK:(c + 1) * CHUNK, :] = dot3(e["qd"], x) + dot3(e["inner"], new)
            states[h] = e["decay"] * x + dot3(e["kd"], new, TN)

    for h in range(heads):
        x_send[h] = states[h].astype(BF16)
    x_copy = pltpu.make_async_remote_copy(
        x_send, x_part, x_sem.at[0], x_sem.at[1], device_id=(partner, tp), device_id_type=MESH)
    x_copy.start()
    x_copy.wait_recv()
    for h in range(heads):
        mine = states[h]
        theirs = x_part[h].astype(F32)
        before = jnp.where(p == 0, mine, theirs)
        after = jnp.where(p == 0, theirs, mine)
        after_s = jnp.concatenate([after[:, :HEAD], jnp.zeros((HEAD, HEAD), F32)], axis=1)
        p_send[h] = (dot3(after[:, HEAD:], before) + after_s).astype(BF16)

    def p_copy(k, to, at):
        return pltpu.make_async_remote_copy(
            p_send, p_recv.at[at], p_ssem.at[k], p_rsem.at[k],
            device_id=(to, tp), device_id_type=MESH)

    for k in range(1, ring):
        @pl.when(r + k < ring)
        def _():
            p_copy(k, sp_of(k, 0), r).start()
    pump(relay_gate)
    for k in range(1, ring):
        @pl.when(r - k >= 0)
        def _():
            p_copy(k, sp_of(-k, 0), r - k).wait_recv()
    s_in[...] = jnp.zeros_like(s_in)

    def fold(i, _):
        for h in range(heads):
            got = p_recv[i, h].astype(F32)
            s_in[h] = dot3(got[:, HEAD:], s_in[h]) + got[:, :HEAD]
        return 0

    lax.fori_loop(0, r, fold, 0)
    for h in range(heads):
        lanes = slice(h * HEAD, (h + 1) * HEAD)
        got = x_part[h].astype(F32)
        s = s_in[h]
        s = jnp.where(p == 0, s, dot3(got[:, HEAD:], s) + got[:, :HEAD])
        att = out_scr[h, :, :HEAD] + dot3(out_scr[h, :, HEAD:], s)
        att = att * lax.rsqrt(jnp.mean(att * att, axis=-1, keepdims=True) + EPSILON) * head_gain[...]
        mixed[:, lanes] = (att * silu(gp[:, lanes].astype(F32))).astype(BF16)

    def rows_of(t):
        return pl.ds(pl.multiple_of(t * own_rows, own_rows), own_rows)

    order = [o for o in (2, 3, 1) if o < tps] + list(range(4, tps))
    d_copies = []
    for o in order:
        to = tp_peer(o)
        d_send[o - 1] = dot1(mixed[rows_of(to), :], w_out[...]).astype(BF16)
        copy = pltpu.make_async_remote_copy(
            d_send.at[o - 1], d_recv.at[o - 1], d_ssem.at[o - 1], d_rsem.at[o - 1],
            device_id=(sp, to), device_id_type=MESH)
        copy.start()
        d_copies.append(copy)
    pump(relay_up)
    pump(far_gate)
    total = dot1(mixed[rows_of(tp), :], w_out[...]).astype(BF16).astype(F32)
    for copy in d_copies:
        copy.wait_recv()
    for o in range(1, tps):
        total = total + d_recv[o - 1].astype(F32)
    total = stream[...].astype(F32) + total
    residual[...] = total
    rows_all[rows_of(tp), :] = (
        total * lax.rsqrt(jnp.mean(total * total, axis=-1, keepdims=True) + EPSILON) * feed_gain[...]
    ).astype(BF16)
    e_copies = []
    for o in order:
        copy = pltpu.make_async_remote_copy(
            rows_all.at[rows_of(tp), :], rows_all.at[rows_of(tp), :], e_ssem.at[o - 1], e_rsem.at[o - 1],
            device_id=(sp, tp_peer(o)), device_id_type=MESH)
        copy.start()
        e_copies.append(copy)
    pump(down_own)
    for o in order:
        there = rows_all.at[rows_of(lax.rem(tp - o + tps, tps)), :]
        pltpu.make_async_remote_copy(
            there, there, e_ssem.at[o - 1], e_rsem.at[o - 1],
            device_id=(sp, tp_peer(o)), device_id_type=MESH).wait_recv()
    for a in "GU":
        for dr in range(ring):
            for rel in (0, 1):
                need(a, dr, rel)
    for local in locals_:
        local.wait()
    pump(relay_down)

    tile = 128

    def ffn_in(i, _):
        lanes = pl.ds(pl.multiple_of(i * tile, tile), tile)
        both = dot1(rows_all[...], jnp.concatenate([gate_all[:, lanes], up_all[:, lanes]], axis=1))
        hidden[:, lanes] = (silu(both[:, :tile]) * both[:, tile:]).astype(BF16)
        return 0

    lax.fori_loop(0, gate_all.shape[1] // tile, ffn_in, 0)
    pump(late)
    for dr in range(ring):
        for rel in (0, 1):
            need("D", dr, rel)
    dc = down_all.shape[2]
    pack = max(1, 128 // dc)
    wide = pack * dc

    def ffn_out(i, _):
        lanes = pl.ds(pl.multiple_of(i * wide, wide), wide)
        if pack == 1:
            weights = down_all[i]
        else:
            weights = jnp.concatenate([down_all[i * pack + j] for j in range(pack)], axis=1)
        f_part[:, lanes] = dot1(hidden[...], weights).astype(BF16)
        return 0

    lax.fori_loop(0, n // pack, ffn_out, 0)
    f_copies = []
    for o in order:
        copy = pltpu.make_async_remote_copy(
            f_part.at[rows_of(tp_peer(o)), :], f_recv.at[o - 1], f_ssem.at[o - 1], f_rsem.at[o - 1],
            device_id=(sp, tp_peer(o)), device_id_type=MESH)
        copy.start()
        f_copies.append(copy)
    ffn = f_part[rows_of(tp), :].astype(F32)
    for copy in f_copies:
        copy.wait_recv()
    for o in range(1, tps):
        ffn = ffn + f_recv[o - 1].astype(F32)
    result[...] = (residual[...] + ffn).astype(BF16)

    for copy in copies + [x_copy] + d_copies + e_copies + f_copies:
        copy.wait_send()
    for k in range(1, ring):
        @pl.when(r + k < ring)
        def _():
            p_copy(k, sp_of(k, 0), r).wait_send()


def body(n, tps, stream, qp, kp, vp, gp, strength, decay_pre, extra, rate, head_gain, w_out,
         feed_gain, gate_m, up_m, down_m):
    heads, tokens = strength.shape
    own, width = stream.shape
    kr, units = gate_m.shape
    ring = n // 2
    groups = messages(ring)
    count = sum(len(g) for g in groups)
    dma = pltpu.SemaphoreType.DMA
    vmem = pl.BlockSpec(memory_space=pltpu.VMEM)
    hbm = pl.BlockSpec(memory_space=pl.ANY)
    peers = max(1, tps - 1)
    return pl.pallas_call(
        functools.partial(kernel, n, tps, groups),
        out_shape=jax.ShapeDtypeStruct((own, width), BF16),
        in_specs=[vmem] * 12 + [hbm] * 3,
        out_specs=vmem,
        scratch_shapes=[
            pltpu.VMEM((kr * n, units), BF16),
            pltpu.VMEM((kr * n, units), BF16),
            pltpu.VMEM((n,) + down_m.shape, BF16),
            pltpu.VMEM((heads, tokens, 2 * HEAD), F32),
            pltpu.VMEM((heads, HEAD, 2 * HEAD), BF16),
            pltpu.VMEM((heads, HEAD, 2 * HEAD), BF16),
            pltpu.VMEM((heads, HEAD, 2 * HEAD), BF16),
            pltpu.VMEM((ring, heads, HEAD, 2 * HEAD), BF16),
            pltpu.VMEM((heads, HEAD, HEAD), F32),
            pltpu.VMEM((tokens, heads * HEAD), BF16),
            pltpu.VMEM((peers, own, width), BF16),
            pltpu.VMEM((peers, own, width), BF16),
            pltpu.VMEM((own, width), F32),
            pltpu.VMEM((tokens, width), BF16),
            pltpu.VMEM((tokens, units), BF16),
            pltpu.VMEM((tokens, width), BF16),
            pltpu.VMEM((peers, own, width), BF16),
            dma((count,)), dma((count,)), dma((3,)), dma((2,)), dma((ring,)), dma((ring,)),
            dma((peers,)), dma((peers,)), dma((peers,)), dma((peers,)), dma((peers,)), dma((peers,)),
        ],
        compiler_params=pltpu.CompilerParams(
            collective_id=0, has_side_effects=True, vmem_limit_bytes=60 * 1024 * 1024),
    )(stream, qp, kp, vp, gp, strength, decay_pre, extra, rate[:, None], head_gain[None, :], w_out,
      feed_gain[None, :], gate_m, up_m, down_m)


def solution(mesh):
    placed = (
        P(("sp", "tp"), None),
        P("sp", "tp"),
        P("sp", "tp"),
        P("sp", "tp"),
        P("sp", "tp"),
        P("tp", "sp"),
        P("tp", "sp"),
        P("tp", "sp"),
        P("tp"),
        P(),
        P("tp", None),
        P(),
        P("sp", "tp"),
        P("sp", "tp"),
        P("tp", "sp"),
    )
    return jax.shard_map(
        functools.partial(body, mesh.shape["sp"], mesh.shape["tp"]),
        mesh=mesh, in_specs=placed, out_specs=P(("sp", "tp"), None), check_vma=False,
    )
```

time: 553 us -> 274 us (0.50)
  waiting for transfers between devices: 364 us -> 0 us
  Pallas kernels: 0 us -> 266 us
  other arithmetic: 74.1 us -> 0 us
  matrix products: 60.9 us -> 0 us
  starting transfers between devices: 34.5 us -> 0 us
  between operations: 13.7 us -> 0.01 us
    all_gather x4 -> x0, waiting for transfers between devices: 291 us -> none  [the longest x1 94.5 us: feed_forward(): lax.all_gather(gate_matrix, 'sp', axis=0, tiled=True)]
    pallas_call x0 -> x1, Pallas kernels: none -> 266 us  [body(): pl.pallas_call(functools.partial(kernel, n, tps, groups), out_shape=jax.S...]
    another operation x5 -> x0, other arithmetic: 60.1 us -> none  [the longest x2 59.6 us: block_correction(): lax.linalg.triangular_solve(system, right_side, left_side=True, lower=Tru...]
    dot_general x61 -> x0, matrix products: 60.1 us -> none  [the longest x1 11.3 us: feed_forward(): return jnp.dot(hidden, down_whole, preferred_element_type=jnp.float32)]
    reduce_scatter x2 -> x0, waiting for transfers between devices: 58.3 us -> none  [the longest x1 31.9 us: body(): lax.psum_scatter(jnp.dot(mixed, head_output_matrix, preferred_element_typ...]
    ppermute x7 -> x0, starting transfers between devices: 34.2 us -> none  [from_behind(): return lax.ppermute(value, axis, pairs)]
    ppermute x7 -> x0, waiting for transfers between devices: 13.4 us -> none  [from_behind(): return lax.ppermute(value, axis, pairs)]
  transfers between devices with their start and end apart: 13 -> 0, of which waited for: 13 -> 0; matrix products, arithmetic and copies ran while one was open for 1% -> 0% of each run, Pallas kernels for 0% -> 0%
where the time goes in v1:
time: 274 us; the launch traced here: 269 us
  Pallas kernels  266 us (97%)
  local copies, waits for them, and re-layouts  3.07 us (1%)
    pallas_call x1, Pallas kernels, body(): pl.pallas_call(functools.partial(kernel, n, tps, groups), out_shape=jax.S...  266 us

profile of v1, /device:TPU:0, one launch (start us, length us, event | category | flops | bytes accessed | tf_op | source)
XLA Modules:
  0.0 269.0 jit_solution(2635605106033840779)
XLA Ops:
  0.0 0.0 copy-start
  0.0 0.7 copy-done
  0.7 0.6 copy.16.rate
  1.3 265.9 %shard_map.145 = bf16[96,2048]{1,0:T(8,128)(2,1)} custom-call(bf16[96,2048]{1,0:T(8,128)(2,1)} %stream.1, bf16[384,256]{1,0:T(8,128)(2,1)} %qp.1, bf16[384,256]{1,0:T(8,128)(2,1)} %kp.1, bf16[384,256]{1,0:T(8,128)(2,1)} %vp.1, bf16[384,256]{1,0:T(8,128)(2,1)} %gp.1, bf16[2,384]{1,0:T(2,128)(2,1)} %strength.1, bf16[2,384]{1,0:T(2,128)(2,1)} %decay_pre.1, ...), custom_call_target="tpu_custom_call" | custom-call | tf_op jit(solution)/shard_map/pallas_call | solution.py:383
  267.2 1.8 copy.18
Async XLA Ops:
  0.0 0.7 copy-start

commit v2 on v1

--- a/solution.py
+++ b/solution.py
@@ -38,34 +38,36 @@
 
 
 def messages(ring):
-    half = ring // 2
-    first, relay_gate, relay_up, relay_down, late = [], [], [], [], []
-    for a in "GU":
-        for way in "RLY":
-            first.append((a, 0, 0, way))
-    for k in range(2, half + 1):
-        relay_gate.append(("G", -(k - 1), 0, "R"))
-        if k < half:
-            relay_gate.append(("G", k - 1, 0, "L"))
-    for k in range(1, half):
-        relay_gate.append(("G", -k, 0, "Y"))
-        relay_gate.append(("G", k, 0, "Y"))
-    far_gate = [("G", half, 0, "Y")] if half else []
-    for k in range(1, half + 1):
-        for rel in (1, 0):
-            if (k > 1 or rel == 1) and (k < half or rel == 0):
-                relay_up.append(("U", -(k - 1), rel, "R"))
-            if (k > 1 or rel == 1) and (k < half or rel == 1):
-                relay_up.append(("U", k - 1, rel, "L"))
-    down_own = [("D", 0, 0, way) for way in "RLY"]
-    for k in range(1, half + 1):
-        for rel in (1, 0):
-            if (k > 1 or rel == 1) and k < half:
-                relay_down.append(("D", -(k - 1), rel, "R"))
-            if (k > 1 or rel == 1) and (k < half or rel == 0):
-                relay_down.append(("D", k - 1, rel, "L"))
-    late.append(("D", half, 0, "Y"))
-    return first, relay_gate, far_gate, relay_up, down_own, relay_down, late
+    own_z = [(a, 0, 0, way) for a in "GU" for way in "RL"]
+    own_y = [(a, 0, 0, "Y") for a in "GU"]
+    first = own_z + own_y
+    down_y = [("D", 0, 0, "Y")]
+
+    def relay(a, j, skip_y=False):
+        out = []
+        if j < ring - 1:
+            out += [(a, -j, 0, "R"), (a, j, 0, "L")]
+        if not skip_y:
+            out += [(a, -j, 0, "Y"), (a, j, 0, "Y")]
+        return out
+
+    early, middle, later, last = [], [], [], []
+    if ring > 1:
+        early = relay("G", 1)
+        middle = relay("U", 1)
+        for j in range(2, ring):
+            later += relay("G", j) + relay("U", j)
+            if j == 2:
+                later += [("D", 0, 0, "R"), ("D", 0, 0, "L")]
+        if ring == 2:
+            later += [("D", 0, 0, "R"), ("D", 0, 0, "L")]
+        later += [("D", 0, 1, "R"), ("D", 0, 1, "L")]
+        later += relay("D", 1, skip_y=True)
+        for j in range(2, ring):
+            last += relay("D", j)
+    else:
+        first = own_y
+    return first, down_y, early, middle, later, last
 
 
 def kernel(
@@ -112,11 +114,14 @@
     arrival = {}
     for (a, dr, rel, way) in flat:
         to = {"R": (dr - 1, rel), "L": (dr + 1, rel), "Y": (dr, 1 - rel)}[way]
-        key = (a, to[0] % ring, to[1])
+        key = (a, to[0], to[1])
         assert key not in arrival
         arrival[key] = number[(a, dr, rel, way)]
     waited = set()
     copies = []
+
+    def exists(dr):
+        return (r + dr >= 0) & (r + dr < ring)
 
     def slot(a, dr, rel):
         s = sp_of(dr, rel)
@@ -128,33 +133,49 @@
     inputs = {"G": gate_in, "U": up_in, "D": down_in}
 
     def need(a, dr, rel):
-        dr = dr % ring
         key = (a, dr, rel)
         if (dr == 0 and rel == 0) or key in waited:
             return
         waited.add(key)
         m = arrival[key]
-        here = slot(*key)
-        pltpu.make_async_remote_copy(
-            here, here, w_send.at[m], w_recv.at[m], device_id=(partner, tp), device_id_type=MESH
-        ).wait_recv()
+
+        @pl.when(exists(dr))
+        def _():
+            here = slot(*key)
+            pltpu.make_async_remote_copy(
+                here, here, w_send.at[m], w_recv.at[m], device_id=(partner, tp), device_id_type=MESH
+            ).wait_recv()
+
+    def outgoing(message):
+        a, dr, rel, way = message
+        m = number[message]
+        return pltpu.make_async_remote_copy(
+            inputs[a] if dr == 0 and rel == 0 else slot(a, dr, rel),
+            slot(a, dr, rel),
+            w_send.at[m], w_recv.at[m],
+            device_id=(where[way], tp), device_id_type=MESH,
+        )
+
+    def goes(message):
+        ahead = {"R": r + 1 < ring, "L": r >= 1, "Y": r >= 0}[message[3]]
+        return exists(message[1]) & ahead
 
     def pump(group):
         for message in group:
-            a, dr, rel, way = message
-            need(a, dr, rel)
-            own = dr % ring == 0 and rel == 0
-            m = number[message]
-            copy = pltpu.make_async_remote_copy(
-                inputs[a] if own else slot(a, dr % ring, rel),
-                slot(a, dr % ring, rel),
-                w_send.at[m], w_recv.at[m],
-                device_id=(where[way], tp), device_id_type=MESH,
-            )
-            copy.start()
-            copies.append(copy)
-
-    first, relay_gate, far_gate, relay_up, down_own, relay_down, late = groups
+            need(*message[:3])
+
+            @pl.when(goes(message))
+            def _():
+                outgoing(message).start()
+
+            copies.append(message)
+
+    def need_all(a):
+        for dr in sorted(range(1 - ring, ring), key=abs):
+            for rel in (0, 1):
+                need(a, dr, rel)
+
+    first, down_y, early, middle, later, last_group = groups
     pump(first)
     locals_ = []
     for i, a in enumerate("GUD"):
@@ -232,6 +253,7 @@
     x_copy = pltpu.make_async_remote_copy(
         x_send, x_part, x_sem.at[0], x_sem.at[1], device_id=(partner, tp), device_id_type=MESH)
     x_copy.start()
+    pump(down_y)
     x_copy.wait_recv()
     for h in range(heads):
         mine = states[h]
@@ -250,7 +272,7 @@
         @pl.when(r + k < ring)
         def _():
             p_copy(k, sp_of(k, 0), r).start()
-    pump(relay_gate)
+    pump(early)
     for k in range(1, ring):
         @pl.when(r - k >= 0)
         def _():
@@ -286,8 +308,7 @@
             device_id=(sp, to), device_id_type=MESH)
         copy.start()
         d_copies.append(copy)
-    pump(relay_up)
-    pump(far_gate)
+    pump(middle)
     total = dot1(mixed[rows_of(tp), :], w_out[...]).astype(BF16).astype(F32)
     for copy in d_copies:
         copy.wait_recv()
@@ -305,19 +326,16 @@
             device_id=(sp, tp_peer(o)), device_id_type=MESH)
         copy.start()
         e_copies.append(copy)
-    pump(down_own)
     for o in order:
         there = rows_all.at[rows_of(lax.rem(tp - o + tps, tps)), :]
         pltpu.make_async_remote_copy(
             there, there, e_ssem.at[o - 1], e_rsem.at[o - 1],
             device_id=(sp, tp_peer(o)), device_id_type=MESH).wait_recv()
-    for a in "GU":
-        for dr in range(ring):
-            for rel in (0, 1):
-                need(a, dr, rel)
+    pump(later)
+    need_all("G")
+    need_all("U")
     for local in locals_:
         local.wait()
-    pump(relay_down)
 
     tile = 128
 
@@ -328,10 +346,8 @@
         return 0
 
     lax.fori_loop(0, gate_all.shape[1] // tile, ffn_in, 0)
-    pump(late)
-    for dr in range(ring):
-        for rel in (0, 1):
-            need("D", dr, rel)
+    pump(last_group)
+    need_all("D")
     dc = down_all.shape[2]
     pack = max(1, 128 // dc)
     wide = pack * dc
@@ -360,7 +376,11 @@
         ffn = ffn + f_recv[o - 1].astype(F32)
     result[...] = (residual[...] + ffn).astype(BF16)
 
-    for copy in copies + [x_copy] + d_copies + e_copies + f_copies:
+    for message in copies:
+        @pl.when(goes(message))
+        def _():
+            outgoing(message).wait_send()
+    for copy in [x_copy] + d_copies + e_copies + f_copies:
         copy.wait_send()
     for k in range(1, ring):
         @pl.when(r + k < ring)

time: 274 us -> 214 us (0.78); the launches traced: 269 us -> 213 us
  Pallas kernels: 266 us -> 210 us
    pallas_call x1, Pallas kernels: 266 us -> 210 us  [body(): pl.pallas_call(functools.partial(kernel, n, tps, groups), out_shape=jax.S...]
where the time goes in v2:
time: 214 us; the launch traced here: 213 us
  Pallas kernels  210 us (98%)
  local copies, waits for them, and re-layouts  3.07 us (1%)
    pallas_call x1, Pallas kernels, body(): pl.pallas_call(functools.partial(kernel, n, tps, groups), out_shape=jax.S...  210 us

profile of v2, /device:TPU:0, one launch (start us, length us, event | category | flops | bytes accessed | tf_op | source)
XLA Modules:
  0.0 213.5 jit_solution(2801789167626529858)
XLA Ops:
  0.0 0.0 copy-start
  0.0 0.7 copy-done
  0.7 0.6 copy.16.rate
  1.3 210.4 %shard_map.145 = bf16[96,2048]{1,0:T(8,128)(2,1)} custom-call(bf16[96,2048]{1,0:T(8,128)(2,1)} %stream.1, bf16[384,256]{1,0:T(8,128)(2,1)} %qp.1, bf16[384,256]{1,0:T(8,128)(2,1)} %kp.1, bf16[384,256]{1,0:T(8,128)(2,1)} %vp.1, bf16[384,256]{1,0:T(8,128)(2,1)} %gp.1, bf16[2,384]{1,0:T(2,128)(2,1)} %strength.1, bf16[2,384]{1,0:T(2,128)(2,1)} %decay_pre.1, ...), custom_call_target="tpu_custom_call" | custom-call | tf_op jit(solution)/shard_map/pallas_call | solution.py:403
  211.7 1.8 copy.18
Async XLA Ops:
  0.0 0.7 copy-start
